TPU v7x, 32 devices: a whole 2x2x4 slice. The times are simulated.
32 devices in a mesh: gr: 2 (over x), fs: 4 (over z), tp: 4 (over y, core).
Axes of the slice: x: 2, y: 2, z: 4, core: 2. Of those that a mesh axis runs over, the one named last changes fastest.
Arguments:
- prompt: bfloat16 [4096, 2048], P(('gr', 'fs', 'tp')), may hold values from -6 to 6
- train_gate: float32 [16, 2048, 256], P(None, ('gr', 'fs'), 'tp'), may hold values from -0.125 to 0.125
- train_up: float32 [16, 2048, 256], P(None, ('gr', 'fs'), 'tp'), may hold values from -0.125 to 0.125
- train_down: float32 [16, 256, 2048], P(None, 'tp', ('gr', 'fs')), may hold values from -0.375 to 0.375
- train_shared_gate: float32 [2048, 256], P(('gr', 'fs'), 'tp'), may hold values from -0.125 to 0.125
- train_shared_up: float32 [2048, 256], P(('gr', 'fs'), 'tp'), may hold values from -0.125 to 0.125
- train_shared_down: float32 [256, 2048], P('tp', ('gr', 'fs')), may hold values from -0.375 to 0.375
- norm_gain: float32 [2048], P(('gr', 'fs')), may hold values from 0.1 to 1.9
- expert_ids: int32 [4096, 8], P(('gr', 'fs', 'tp')), may hold values from 0 to 15, all different within a row; in each aligned block of 128 rows (0 to 127, 128 to 255, ...) at most 65 rows name the same one
- route_weight: float32 [4096, 8], P(('gr', 'fs', 'tp')), may hold values from 0.05 to 0.6
Outputs:
- serve_gate: bfloat16 [16, 2048, 256], P(('fs', 'tp'))
- serve_up: bfloat16 [16, 2048, 256], P(('fs', 'tp'))
- serve_down: bfloat16 [16, 256, 2048], P(('fs', 'tp'))
- serve_shared_gate: bfloat16 [2048, 256], P(None, 'tp')
- serve_shared_up: bfloat16 [2048, 256], P(None, 'tp')
- serve_shared_down: bfloat16 [256, 2048], P('tp')
- mixed_out: bfloat16 [4096, 2048], P(('gr', 'fs', 'tp'))
Inputs may be any that keep to these rules, and one draw needn't show every extreme that they name: `expert_ids`: each row names 8 different experts. Among the rows of one device no expert is named by more than 65 rows, and in some device's rows one expert is named by exactly 65.
All inputs are finite; a program needn't handle non-finite values.
Results may differ from a plain program's by a relative error of at most 0.012.
Values may be sent and summed in bfloat16 or wider, within the bound.
No kernel may reach another device: no remote copies, remote signals or barrier semaphores. Data moves between devices by JAX's collectives and lax.ppermute only.
A program may use at most 128 MiB of HBM per device.

v0:
```python
import jax
import jax.numpy as jnp
from jax import lax
from jax.sharding import PartitionSpec as P

eps_norm = 1e-06


def regroup(stacked, lowered):
    stacked = lax.all_to_all(
        lax.all_to_all(stacked, "fs", split_axis=0, concat_axis=2, tiled=True),
        "tp",
        split_axis=0,
        concat_axis=3,
        tiled=True,
    )
    lowered = lax.all_to_all(
        lax.all_to_all(lowered, "fs", split_axis=0, concat_axis=2, tiled=True),
        "tp",
        split_axis=0,
        concat_axis=1,
        tiled=True,
    )
    return (stacked, lowered)


def body(
    prompt,
    train_gate,
    train_up,
    train_down,
    train_shared_gate,
    train_shared_up,
    train_shared_down,
    norm_gain,
    expert_ids,
    route_weight,
):
    gain_col = norm_gain[:, None]
    stacked = jnp.stack((train_gate * gain_col[None], train_up * gain_col[None]), axis=1).astype(
        jnp.bfloat16
    )
    lowered = train_down.astype(jnp.bfloat16)
    stacked, lowered = regroup(stacked, lowered)
    stacked, lowered = (
        lax.all_gather(stacked, "gr", axis=2, tiled=True),
        lax.all_gather(lowered, "gr", axis=2, tiled=True),
    )
    serve_gate = stacked[:, 0]
    serve_up = stacked[:, 1]
    serve_shared_gate, serve_shared_up, serve_shared_down = (
        lax.all_gather(
            (train_shared_gate * gain_col).astype(jnp.bfloat16), ("gr", "fs"), axis=0, tiled=True
        ),
        lax.all_gather(
            (train_shared_up * gain_col).astype(jnp.bfloat16), ("gr", "fs"), axis=0, tiled=True
        ),
        lax.all_gather(train_shared_down.astype(jnp.bfloat16), ("gr", "fs"), axis=1, tiled=True),
    )
    widened = prompt.astype(jnp.float32)
    normed = (
        widened * lax.rsqrt(jnp.mean(widened * widened, axis=-1, keepdims=True) + eps_norm)
    ).astype(jnp.bfloat16)
    block_rows = lax.all_gather(normed, "tp", axis=0, tiled=True)
    gate_val = jnp.dot(block_rows, serve_shared_gate, preferred_element_type=jnp.float32)
    up_val = jnp.dot(block_rows, serve_shared_up, preferred_element_type=jnp.float32)
    shared_act = (jax.nn.silu(gate_val) * up_val).astype(jnp.bfloat16)
    shared_sum = lax.psum_scatter(
        jnp.dot(shared_act, serve_shared_down, preferred_element_type=jnp.float32).astype(
            jnp.bfloat16
        ),
        "tp",
        scatter_dimension=0,
        tiled=True,
    ).astype(jnp.float32)
    row_count = prompt.shape[0]
    top_count = expert_ids.shape[1]
    model_width = prompt.shape[1]
    expert_count = lax.axis_size("fs") * lax.axis_size("tp")
    capacity = row_count * top_count // expert_count + 1
    flat_ids = expert_ids.reshape(-1)
    onehot = (flat_ids[:, None] == jnp.arange(expert_count, dtype=jnp.int32)[None, :]).astype(
        jnp.int32
    )
    earlier = jnp.cumsum(onehot, axis=0) - onehot
    places = jnp.sum(earlier * onehot, axis=1)
    slot_ids = (flat_ids * capacity + places).reshape(row_count, top_count)
    slot_range = jnp.arange(expert_count * capacity, dtype=jnp.int32)
    dispatch = jnp.any(slot_range[:, None, None] == slot_ids[None, :, :], axis=-1).astype(
        jnp.bfloat16
    )
    outgoing = jnp.dot(dispatch, normed, preferred_element_type=jnp.float32).astype(jnp.bfloat16)
    outgoing = outgoing.reshape(expert_count, capacity, model_width)
    arrived = lax.all_to_all(outgoing, ("fs", "tp"), split_axis=0, concat_axis=0, tiled=True)
    source_count, slot_count, width_here = arrived.shape
    arrived_rows = arrived.reshape(source_count * slot_count, width_here)
    gate_val = jnp.dot(arrived_rows, serve_gate[0], preferred_element_type=jnp.float32)
    up_val = jnp.dot(arrived_rows, serve_up[0], preferred_element_type=jnp.float32)
    hidden = (jax.nn.silu(gate_val) * up_val).astype(jnp.bfloat16)
    result = jnp.dot(hidden, lowered[0], preferred_element_type=jnp.float32).astype(jnp.bfloat16)
    result = result.reshape(source_count, slot_count, width_here)
    returned = lax.all_to_all(result, ("fs", "tp"), split_axis=0, concat_axis=0, tiled=True)
    picked = returned.reshape(expert_count * capacity, model_width)[slot_ids]
    routed = jnp.sum(route_weight[:, :, None] * picked.astype(jnp.float32), axis=1)
    mixed_out = (routed + shared_sum).astype(jnp.bfloat16)
    return (
        serve_gate,
        serve_up,
        lowered,
        serve_shared_gate,
        serve_shared_up,
        serve_shared_down,
        mixed_out,
    )


def solution(mesh):
    placed = (
        P(("gr", "fs", "tp"), None),
        P(None, ("gr", "fs"), "tp"),
        P(None, ("gr", "fs"), "tp"),
        P(None, "tp", ("gr", "fs")),
        P(("gr", "fs"), "tp"),
        P(("gr", "fs"), "tp"),
        P("tp", ("gr", "fs")),
        P(("gr", "fs")),
        P(("gr", "fs", "tp"), None),
        P(("gr", "fs", "tp"), None),
    )
    return jax.shard_map(
        body,
        mesh=mesh,
        in_specs=placed,
        out_specs=(
            P(("fs", "tp"), None, None),
            P(("fs", "tp"), None, None),
            P(("fs", "tp"), None, None),
            P(None, "tp"),
            P(None, "tp"),
            P("tp", None),
            P(("gr", "fs", "tp"), None),
        ),
        check_vma=False,
    )
```

profile of v0, /device:TPU:0, one launch (start us, length us, event | category | flops | bytes accessed | tf_op | source)
XLA Modules:
  0.0 467.0 jit_solution(16509403626507638138)
XLA Ops:
  10.1 6.5 %all-to-all-start.2 = ((bf16[16,64,256]{2,1,0:T(8,128)(2,1)}), bf16[16,64,256]{2,1,0:T(8,128)(2,1)S(1)}, u32[]{:S(2)}, u32[]{:S(2)}) async-start(bf16[16,64,256]{2,1,0:T(8,128)(2,1)} %convert_element_type.51), calls=%async_computation.2 | async-start | bytes 1048576 | tf_op jit(solution)/shard_map/all_to_all | solution.py:18
  19.4 11.6 %all-to-all-done.2 = bf16[16,64,256]{2,1,0:T(8,128)(2,1)S(1)} async-done(((bf16[16,64,256]{2,1,0:T(8,128)(2,1)}), bf16[16,64,256]{2,1,0:T(8,128)(2,1)S(1)}, u32[]{:S(2)}, u32[]{:S(2)}) %all-to-all-start.2) | async-done | bytes 524320 | tf_op jit(solution)/shard_map/all_to_all | solution.py:18
  31.1 3.5 all-to-all-start
  34.9 4.5 reduce-window.6
  40.9 18.9 %all-to-all-done = bf16[16,2,256,64]{2,3,1,0:T(8,128)(2,1)S(1)} async-done(((bf16[16,2,256,64]{2,3,1,0:T(8,128)(2,1)}), bf16[16,2,256,64]{2,3,1,0:T(8,128)(2,1)S(1)}, u32[]{:S(2)}, u32[]{:S(2)}) %all-to-all-start) | async-done | bytes 1048608 | tf_op jit(solution)/shard_map/all_to_all | solution.py:11
  63.5 3.8 fusion.1
  68.4 3.7 all-to-all-done.3
  72.1 3.5 all-to-all-start.1
  79.0 4.4 reshape.67
  83.4 6.6 %all-to-all-done.1 = bf16[4,2,1024,64]{2,3,1,0:T(8,128)(2,1)S(1)} async-done(((bf16[4,2,1024,64]{2,3,1,0:T(8,128)(2,1)}), bf16[4,2,1024,64]{2,3,1,0:T(8,128)(2,1)S(1)}, u32[]{:S(2)}, u32[]{:S(2)}) %all-to-all-start.1) | async-done | bytes 1048608 | tf_op jit(solution)/shard_map/all_to_all | solution.py:10
  90.0 4.6 all-to-all-start.4
  96.5 84.7 %all-to-all-done.4 = bf16[16,65,2048]{2,1,0:T(8,128)(2,1)} async-done(((bf16[16,65,2048]{2,1,0:T(8,128)(2,1)}), bf16[16,65,2048]{2,1,0:T(8,128)(2,1)}, u32[]{:S(2)}, u32[]{:S(2)}) %all-to-all-start.4) | async-done | bytes 4259872 | tf_op jit(solution)/shard_map/all_to_all | solution.py:94
  181.2 4.4 reshape.68
  185.6 5.0 %fusion.14 = f32[1040,256]{1,0:T(8,128)} fusion(bf16[1040,2048]{1,0:T(8,128)(2,1)} %reshape.68, bf16[1,2,2048,256]{2,3,1,0:T(8,128)(2,1)} %all-gather.4.cloned.1.call-done), kind=kOutput, calls=%fused_computation.24 | convolution fusion | flops 1090519040 | bytes 6373376 | tf_op jit(solution)/shard_map/dot_general | solution.py:97
  190.6 9.2 %convolution_convert_fusion = bf16[1040,2048]{1,0:T(8,128)(2,1)} fusion(bf16[1040,2048]{1,0:T(8,128)(2,1)} %reshape.68, f32[1040,256]{1,0:T(8,128)} %fusion.14, bf16[1,256,2048]{2,1,0:T(8,128)(2,1)} %all-gather.6.cloned.1.call-done, bf16[1,2,2048,256]{2,3,1,0:T(8,128)(2,1)S(1)} %copy-done.1), kind=kOutput, calls=%fused_computation.3 | convolution fusion | flops 2184765440 | bytes 11681792 | tf_op jit(solution)/shard_map/dot_general | solution.py:100
  199.9 4.4 reshape.69
  204.3 21.9 %all-to-all-start.5 = ((bf16[16,65,2048]{2,1,0:T(8,128)(2,1)}), bf16[16,65,2048]{2,1,0:T(8,128)(2,1)}, u32[]{:S(2)}, u32[]{:S(2)}) async-start(bf16[16,65,2048]{2,1,0:T(8,128)(2,1)} %reshape.69), calls=%async_computation.5 | async-start | bytes 9437184 | tf_op jit(solution)/shard_map/all_to_all | solution.py:102
  226.9 127.8 %all_gather.20 = bf16[2048,64]{0,1:T(8,128)(2,1)S(1)} all-gather(bf16[256,64]{0,1:T(8,128)(2,1)S(1)} %get-tuple-element.40), channel_id=1, replica_groups=mesh['gr'=2,'fs'=4,'tp'=4] {'gr','fs'}, dimensions={0}, use_global_device_ids=true | all-gather | bytes 294912 | tf_op jit(solution)/shard_map/all_gather | solution.py:52
  354.8 31.4 %all_gather.21 = bf16[2048,64]{0,1:T(8,128)(2,1)S(1)} all-gather(bf16[256,64]{0,1:T(8,128)(2,1)S(1)} %get-tuple-element.39), channel_id=1, replica_groups=mesh['gr'=2,'fs'=4,'tp'=4] {'gr','fs'}, dimensions={0}, use_global_device_ids=true | all-gather | bytes 294912 | tf_op jit(solution)/shard_map/all_gather | solution.py:55
  386.2 31.3 %all_gather.22 = bf16[64,2048]{1,0:T(8,128)(2,1)S(1)} all-gather(bf16[64,256]{1,0:T(8,128)(2,1)S(1)} %convert_element_type.54), channel_id=1, replica_groups=mesh['gr'=2,'fs'=4,'tp'=4] {'gr','fs'}, dimensions={1}, use_global_device_ids=true | all-gather | bytes 294912 | tf_op jit(solution)/shard_map/all_gather | solution.py:58
  419.8 4.5 convolution_convert_fusion.2
  429.0 4.9 %reshape.70 = bf16[1040,2048]{1,0:T(8,128)(2,1)} reshape(bf16[16,65,2048]{2,1,0:T(8,128)(2,1)} %all-to-all-done.5) | data formatting | bytes 8519680 | tf_op jit(solution)/shard_map/reshape | solution.py:103
  433.9 11.6 %gather_fusion = bf16[1024,2048]{1,0:T(8,128)(2,1)} fusion(bf16[1040,2048]{1,0:T(8,128)(2,1)} %reshape.70, s32[1024]{0:T(1024)S(1)} %broadcast_clamp_fusion), kind=kCustom, calls=%fused_computation | custom fusion | bytes 8392704 | tf_op jit(solution)/shard_map/gather | solution.py:103
  445.5 6.6 %fusion = f32[128,2048]{1,0:T(8,128)S(1)} fusion(bf16[1024,2048]{1,0:T(8,128)(2,1)} %gather_fusion, f32[128,8]{1,0:T(8,128)S(1)} %copy.65), kind=kLoop, calls=%fused_computation.2 | loop fusion | flops 6029312 | bytes 5246976 | tf_op jit(solution)/shard_map/reduce_sum | solution.py:104
  (75 shorter events, 31.7 us)
Async XLA Ops:
  10.1 24.5 %copy-start.8 = (s32[128,8]{0,1:T(8,128)S(1)}, s32[128,8]{0,1:T(8,128)}, u32[]{:S(2)}) copy-start(s32[128,8]{0,1:T(8,128)} %param.18) | copy-start | bytes 12292
  10.1 21.0 %all-to-all-start.2 = ((bf16[16,64,256]{2,1,0:T(8,128)(2,1)}), bf16[16,64,256]{2,1,0:T(8,128)(2,1)S(1)}, u32[]{:S(2)}, u32[]{:S(2)}) async-start(bf16[16,64,256]{2,1,0:T(8,128)(2,1)} %convert_element_type.51), calls=%async_computation.2 | async-start | bytes 1048576 | tf_op jit(solution)/shard_map/all_to_all | solution.py:18
  18.4 45.0 %copy-start.2 = (bf16[128,2048]{1,0:T(8,128)(2,1)S(1)}, bf16[128,2048]{1,0:T(8,128)(2,1)}, u32[]{:S(2)}) copy-start(bf16[128,2048]{1,0:T(8,128)(2,1)} %param.10) | copy-start | bytes 1572868
  31.1 28.8 %all-to-all-start = ((bf16[16,2,256,64]{2,3,1,0:T(8,128)(2,1)}), bf16[16,2,256,64]{2,3,1,0:T(8,128)(2,1)S(1)}, u32[]{:S(2)}, u32[]{:S(2)}) async-start(bf16[16,2,256,64]{2,3,1,0:T(8,128)(2,1)} %pad_maximum_fusion), calls=%async_computation | async-start | bytes 2097152 | tf_op jit(solution)/shard_map/all_to_all | solution.py:11
  59.8 12.3 %all-to-all-start.3 = ((bf16[4,64,1024]{2,1,0:T(8,128)(2,1)}), bf16[4,64,1024]{2,1,0:T(8,128)(2,1)S(1)}, u32[]{:S(2)}, u32[]{:S(2)}) async-start(bf16[4,64,1024]{2,1,0:T(8,128)(2,1)} %bitcast.28), calls=%async_computation.3 | async-start | bytes 1048576 | tf_op jit(solution)/shard_map/all_to_all | solution.py:17
  72.1 6.9 %copy-start.3 = (bf16[4,64,1024]{2,1,0:T(8,128)(2,1)}, bf16[4,64,1024]{2,1,0:T(8,128)(2,1)S(1)}, u32[]{:S(2)}) copy-start(bf16[4,64,1024]{2,1,0:T(8,128)(2,1)S(1)} %all-to-all-done.3) | copy-start | bytes 1572868
  72.1 17.9 %all-to-all-start.1 = ((bf16[4,2,1024,64]{2,3,1,0:T(8,128)(2,1)}), bf16[4,2,1024,64]{2,3,1,0:T(8,128)(2,1)S(1)}, u32[]{:S(2)}, u32[]{:S(2)}) async-start(bf16[4,2,1024,64]{2,3,1,0:T(8,128)(2,1)} %bitcast.26), calls=%async_computation.1 | async-start | bytes 2097152 | tf_op jit(solution)/shard_map/all_to_all | solution.py:10
  75.8 7.7 %copy-start = (bf16[128,2048]{1,0:T(8,128)(2,1)}, bf16[128,2048]{1,0:T(8,128)(2,1)S(1)}, u32[]{:S(2)}) copy-start(bf16[128,2048]{1,0:T(8,128)(2,1)S(1)} %fusion.10) | copy-start | bytes 1572868
  90.0 91.2 %all-to-all-start.4 = ((bf16[16,65,2048]{2,1,0:T(8,128)(2,1)}), bf16[16,65,2048]{2,1,0:T(8,128)(2,1)}, u32[]{:S(2)}, u32[]{:S(2)}) async-start(bf16[16,65,2048]{2,1,0:T(8,128)(2,1)} %reshape.67), calls=%async_computation.4 | async-start | bytes 9437184 | tf_op jit(solution)/shard_map/all_to_all | solution.py:94
  94.6 91.1 %all-gather.4.cloned.1.call-start = ((), (), s32[]{:S(2)}) async-start(), calls=%async_computation.7 | async-start | bytes 3145728 | tf_op jit(solution)/shard_map/all_gather | solution.py:46
  95.7 94.9 %all-gather.6.cloned.1.call-start = ((), (), s32[]{:S(2)}) async-start(), calls=%async_computation.8 | async-start | bytes 1572864 | tf_op jit(solution)/shard_map/all_gather | solution.py:47
  185.6 5.0 %copy-start.1 = (bf16[1,2,2048,256]{2,3,1,0:T(8,128)(2,1)S(1)}, bf16[1,2,2048,256]{2,3,1,0:T(8,128)(2,1)}, u32[]{:S(2)}) copy-start(bf16[1,2,2048,256]{2,3,1,0:T(8,128)(2,1)} %all-gather.4.cloned.1.call-done) | copy-start | bytes 6291460
  204.3 22.6 %copy-start.7 = (f32[64,256]{1,0:T(8,128)S(1)}, f32[64,256]{1,0:T(8,128)}, u32[]{:S(2)}) copy-start(f32[64,256]{1,0:T(8,128)} %param.16) | copy-start | bytes 196612
  204.3 22.6 %copy-start.5 = (f32[256,64]{0,1:T(8,128)S(1)}, f32[256,64]{0,1:T(8,128)}, u32[]{:S(2)}) copy-start(f32[256,64]{0,1:T(8,128)} %param.15) | copy-start | bytes 196612
  204.3 22.6 %copy-start.6 = (f32[256,64]{0,1:T(8,128)S(1)}, f32[256,64]{0,1:T(8,128)}, u32[]{:S(2)}) copy-start(f32[256,64]{0,1:T(8,128)} %param.14) | copy-start | bytes 196612
  204.3 22.6 %copy-start.9 = (f32[256]{0:T(256)S(1)}, f32[256]{0:T(256)}, u32[]{:S(2)}) copy-start(f32[256]{0:T(256)} %param.17) | copy-start | bytes 3076
  204.3 224.7 %all-to-all-start.5 = ((bf16[16,65,2048]{2,1,0:T(8,128)(2,1)}), bf16[16,65,2048]{2,1,0:T(8,128)(2,1)}, u32[]{:S(2)}, u32[]{:S(2)}) async-start(bf16[16,65,2048]{2,1,0:T(8,128)(2,1)} %reshape.69), calls=%async_computation.5 | async-start | bytes 9437184 | tf_op jit(solution)/shard_map/all_to_all | solution.py:102
  226.2 191.3 %all-gather.8.cloned.1.call-start = ((), (), s32[]{:S(2)}) async-start(), calls=%async_computation.9 | async-start | bytes 2621440 | tf_op jit(solution)/shard_map/all_gather | solution.py:64
  226.8 227.7 %reduce-scatter.2.cloned.1.call-start = ((), (), s32[]{:S(2)}) async-start(), calls=%async_computation.10 | async-start | bytes 2621440 | tf_op jit(solution)/shard_map/reduce_scatter | solution.py:68
  417.5 7.1 %copy-start.10 = (f32[128,8]{0,1:T(8,128)S(1)}, f32[128,8]{0,1:T(8,128)}, u32[]{:S(2)}) copy-start(f32[128,8]{0,1:T(8,128)} %param.19) | copy-start | bytes 12292
  445.5 11.0 %copy-start.4 = (bf16[1,256,2048]{2,1,0:T(8,128)(2,1)S(1)}, bf16[1,256,2048]{2,1,0:T(8,128)(2,1)}, u32[]{:S(2)}) copy-start(bf16[1,256,2048]{2,1,0:T(8,128)(2,1)} %all-gather.6.cloned.1.call-done) | copy-start | bytes 3145732
Sparse Core Ops, SparseCore 0:
  97.5 34.2 all-gather.3
  134.0 21.2 all-gather.5
Sparse Core Ops, SparseCore 1:
  228.8 46.7 all-gather.7
  424.5 30.0 reduce-scatter.1
where the time goes:
time: 468 us; the launch traced here: 467 us
  blocking collectives  191 us (41%)
  waiting for transfers between devices  129 us (28%)
  starting transfers between devices  43.8 us (9%)
  local copies, waits for them, and re-layouts  41.3 us (9%)
  matrix products  24.3 us (5%)
  other arithmetic  22.3 us (5%)
  between operations  15.7 us (3%)
    all_gather x1, blocking collectives, body(): lax.all_gather((train_shared_gate * gain_col).astype(jnp.bfloat16), ('gr'...  128 us
    all_to_all x1, waiting for transfers between devices, body(): lax.all_to_all(outgoing, ('fs', 'tp'), split_axis=0, concat_axis=0, tiled...  84.7 us
    all_gather x1, blocking collectives, body(): lax.all_gather((train_shared_up * gain_col).astype(jnp.bfloat16), ('gr',...  31.4 us
    all_gather x1, blocking collectives, body(): lax.all_gather(train_shared_down.astype(jnp.bfloat16), ('gr', 'fs'), axis...  31.3 us
    all_to_all x1, starting transfers between devices, body(): lax.all_to_all(result, ('fs', 'tp'), split_axis=0, concat_axis=0, tiled=T...  21.9 us
    all_to_all x1, waiting for transfers between devices, regroup(): lax.all_to_all(stacked, 'fs', split_axis=0, concat_axis=2, tiled=True)  18.9 us
    all_to_all x1, waiting for transfers between devices, regroup(): lax.all_to_all(lowered, 'fs', split_axis=0, concat_axis=2, tiled=True)  11.6 us
    gather x1, local copies, waits for them, and re-layouts, body(): picked = returned.reshape(expert_count * capacity, model_width)[slot_ids]  11.6 us
  transfers between devices with their start and end apart: 10, of which 6 were waited for; matrix products, arithmetic and copies ran while one was open for 14% of the time, Pallas kernels for 0%

commit v1 on v0

v1 whole, which is shorter than its diff:
```python
import jax
import jax.numpy as jnp
from jax import lax
from jax.sharding import PartitionSpec as P

eps_norm = 1e-06
row_tile = 8


def to_owners(pieces):
    count, kinds, hidden_part, width_part = pieces.shape
    fs, tp = lax.axis_size("fs"), lax.axis_size("tp")
    pieces = lax.all_to_all(pieces, ("fs", "tp"), split_axis=0, concat_axis=0, tiled=True)
    pieces = pieces.reshape(fs, tp, kinds, hidden_part, width_part)
    pieces = pieces.transpose(2, 1, 3, 0, 4).reshape(kinds, tp * hidden_part, fs * width_part)
    return lax.all_gather(pieces, "gr", axis=2, tiled=True)


def dot_last(left, right):
    return lax.dot_general(left, right, (((1,), (1,)), ((), ())), preferred_element_type=jnp.float32)


def gated(rows, gate_up):
    both = dot_last(rows, gate_up)
    hidden = both.shape[1] // 2
    return jax.nn.silu(both[:, :hidden]) * both[:, hidden:]


def dense_mix(normed, expert_ids, route_weight, gate_up, lowered, shared_gate_up, shared_down):
    fs, tp = lax.axis_size("fs"), lax.axis_size("tp")
    expert_count = fs * tp
    row_count, model_width = normed.shape
    named = expert_ids[None, :, :] == jnp.arange(expert_count, dtype=jnp.int32)[:, None, None]
    weights = jnp.sum(jnp.where(named, route_weight[None], 0.0), axis=2)
    high = lax.reduce_precision(weights, 8, 7)
    coded = jnp.stack((high, weights - high)).astype(jnp.bfloat16).reshape(-1)
    extra = -(-coded.size // (model_width * row_tile)) * row_tile
    coded = jnp.pad(coded, (0, extra * model_width - coded.size)).reshape(extra, model_width)
    block = lax.all_gather(jnp.concatenate((normed, coded), axis=0), ("fs", "tp"), axis=0)
    height = row_count + extra
    mine = lax.axis_index("fs") * tp + lax.axis_index("tp")
    sent = block[:, row_count:].reshape(expert_count, -1)[:, : 2 * expert_count * row_count]
    sent = sent.reshape(expert_count, 2, expert_count, row_count)
    own = lax.dynamic_index_in_dim(sent, mine, axis=2, keepdims=False).astype(jnp.float32)
    own = (own[:, 0] + own[:, 1])[:, :, None]
    act = gated(block.reshape(-1, model_width), gate_up).reshape(expert_count, height, -1)
    act = (act[:, :row_count] * own).astype(jnp.bfloat16)
    near = lax.dynamic_slice_in_dim(block, lax.axis_index("fs") * tp, tp, axis=0)
    shared_act = gated(near.reshape(-1, model_width), shared_gate_up).astype(jnp.bfloat16)
    shared_act = shared_act.reshape(tp, height, -1)[:, :row_count]
    placed = jnp.zeros((expert_count, row_count, shared_act.shape[2]), jnp.bfloat16)
    placed = lax.dynamic_update_slice_in_dim(placed, shared_act, lax.axis_index("fs") * tp, axis=0)
    act = jnp.concatenate((act, placed), axis=2).reshape(expert_count * row_count, -1)
    down = jnp.concatenate((lowered, shared_down), axis=0)
    partial = jnp.dot(act, down, preferred_element_type=jnp.float32).astype(jnp.bfloat16)
    return lax.psum_scatter(partial, ("fs", "tp"), scatter_dimension=0, tiled=True)


def sparse_mix(normed, expert_ids, route_weight, gate_up, lowered, shared_gate_up, shared_down):
    block_rows = lax.all_gather(normed, "tp", axis=0, tiled=True)
    shared_act = gated(block_rows, shared_gate_up).astype(jnp.bfloat16)
    shared_sum = lax.psum_scatter(
        jnp.dot(shared_act, shared_down, preferred_element_type=jnp.float32).astype(jnp.bfloat16),
        "tp",
        scatter_dimension=0,
        tiled=True,
    ).astype(jnp.float32)
    row_count, model_width = normed.shape
    top_count = expert_ids.shape[1]
    expert_count = lax.axis_size("fs") * lax.axis_size("tp")
    capacity = row_count * top_count // expert_count + 1
    flat_ids = expert_ids.reshape(-1)
    onehot = (flat_ids[:, None] == jnp.arange(expert_count, dtype=jnp.int32)[None, :]).astype(
        jnp.int32
    )
    earlier = jnp.cumsum(onehot, axis=0) - onehot
    places = jnp.sum(earlier * onehot, axis=1)
    slot_ids = (flat_ids * capacity + places).reshape(row_count, top_count)
    slot_range = jnp.arange(expert_count * capacity, dtype=jnp.int32)
    dispatch = jnp.any(slot_range[:, None, None] == slot_ids[None, :, :], axis=-1).astype(
        jnp.bfloat16
    )
    outgoing = jnp.dot(dispatch, normed, preferred_element_type=jnp.float32).astype(jnp.bfloat16)
    outgoing = outgoing.reshape(expert_count, capacity, model_width)
    arrived = lax.all_to_all(outgoing, ("fs", "tp"), split_axis=0, concat_axis=0, tiled=True)
    source_count, slot_count, width_here = arrived.shape
    arrived_rows = arrived.reshape(source_count * slot_count, width_here)
    hidden = gated(arrived_rows, gate_up).astype(jnp.bfloat16)
    result = jnp.dot(hidden, lowered, preferred_element_type=jnp.float32).astype(jnp.bfloat16)
    result = result.reshape(source_count, slot_count, width_here)
    returned = lax.all_to_all(result, ("fs", "tp"), split_axis=0, concat_axis=0, tiled=True)
    picked = returned.reshape(expert_count * capacity, model_width)[slot_ids]
    routed = jnp.sum(route_weight[:, :, None] * picked.astype(jnp.float32), axis=1)
    return (routed + shared_sum).astype(jnp.bfloat16)


def body(
    prompt,
    train_gate,
    train_up,
    train_down,
    train_shared_gate,
    train_shared_up,
    train_shared_down,
    norm_gain,
    expert_ids,
    route_weight,
):
    widened = prompt.astype(jnp.float32)
    normed = (
        widened * lax.rsqrt(jnp.mean(widened * widened, axis=-1, keepdims=True) + eps_norm)
    ).astype(jnp.bfloat16)
    gained_gate = jnp.swapaxes(train_gate, 1, 2) * norm_gain
    gained_up = jnp.swapaxes(train_up, 1, 2) * norm_gain
    stacked = to_owners(jnp.stack((gained_gate, gained_up), axis=1).astype(jnp.bfloat16))
    lowered = to_owners(train_down.astype(jnp.bfloat16)[:, None])
    shared = jnp.stack(
        (
            train_shared_gate.T * norm_gain,
            train_shared_up.T * norm_gain,
            train_shared_down,
            jnp.zeros_like(train_shared_down),
        )
    ).astype(jnp.bfloat16)
    shared = lax.all_gather(shared, ("gr", "fs"), axis=0)
    shared = shared[:, :3].transpose(1, 2, 0, 3).reshape(3, train_shared_down.shape[0], -1)
    model_width = prompt.shape[1]
    mix = dense_mix if lax.axis_size("fs") * lax.axis_size("tp") <= 2 * expert_ids.shape[1] else sparse_mix
    mixed_out = mix(
        normed,
        expert_ids,
        route_weight,
        stacked.reshape(-1, model_width),
        lowered[0],
        shared[:2].reshape(-1, model_width),
        shared[2],
    )
    return (
        jnp.swapaxes(stacked[:1], 1, 2),
        jnp.swapaxes(stacked[1:], 1, 2),
        lowered,
        shared[0].T,
        shared[1].T,
        shared[2],
        mixed_out,
    )


def solution(mesh):
    placed = (
        P(("gr", "fs", "tp"), None),
        P(None, ("gr", "fs"), "tp"),
        P(None, ("gr", "fs"), "tp"),
        P(None, "tp", ("gr", "fs")),
        P(("gr", "fs"), "tp"),
        P(("gr", "fs"), "tp"),
        P("tp", ("gr", "fs")),
        P(("gr", "fs")),
        P(("gr", "fs", "tp"), None),
        P(("gr", "fs", "tp"), None),
    )
    return jax.shard_map(
        body,
        mesh=mesh,
        in_specs=placed,
        out_specs=(
            P(("fs", "tp"), None, None),
            P(("fs", "tp"), None, None),
            P(("fs", "tp"), None, None),
            P(None, "tp"),
            P(None, "tp"),
            P("tp", None),
            P(("gr", "fs", "tp"), None),
        ),
        check_vma=False,
    )
```

time: 468 us -> 324 us (0.69)
  blocking collectives: 191 us -> 43.9 us
  waiting for transfers between devices: 129 us -> 219 us
  starting transfers between devices: 43.8 us -> 5.29 us
  local copies, waits for them, and re-layouts: 41.3 us -> 15.8 us
  other arithmetic: 22.3 us -> 9.15 us
  matrix products: 24.3 us -> 16.7 us
    all_gather x3 -> x0, blocking collectives: 191 us -> none  [the longest x1 128 us: body(): lax.all_gather((train_shared_gate * gain_col).astype(jnp.bfloat16), ('gr'...]
    all_to_all x6 -> x1, waiting for transfers between devices: 126 us -> 21.5 us  [to_owners(): lax.all_to_all(pieces, ('fs', 'tp'), split_axis=0, concat_axis=0, tiled=T...]
    all_gather x3 -> x4, waiting for transfers between devices: 0.01 us -> 99.4 us  [the longest x1 55.9 us: dense_mix(): lax.all_gather(jnp.concatenate((normed, coded), axis=0), ('fs', 'tp'), ax...]
    reduce_scatter x1, waiting for transfers between devices: 2.4 us -> 97.8 us  [dense_mix(): lax.psum_scatter(partial, ('fs', 'tp'), scatter_dimension=0, tiled=True)]
    all_to_all x0 -> x1, blocking collectives: none -> 43.9 us  [to_owners(): lax.all_to_all(pieces, ('fs', 'tp'), split_axis=0, concat_axis=0, tiled=T...]
    all_to_all x6 -> x1, starting transfers between devices: 43.5 us -> 5.08 us  [to_owners(): lax.all_to_all(pieces, ('fs', 'tp'), split_axis=0, concat_axis=0, tiled=T...]
    reshape x4, local copies, waits for them, and re-layouts: 18.2 us -> 3.54 us  [the longest x2 2.71 us: to_owners(): pieces.transpose(2, 1, 3, 0, 4)]
    gather x1 -> x0, local copies, waits for them, and re-layouts: 11.6 us -> none  [body(): picked = returned.reshape(expert_count * capacity, model_width)[slot_ids]]
  transfers between devices with their start and end apart: 10 -> 6, of which waited for: 6 -> 5; matrix products, arithmetic and copies ran while one was open for 14% -> 9% of each run, Pallas kernels for 0% -> 0%
where the time goes in v1:
time: 324 us
  waiting for transfers between devices  219 us (68%)
  blocking collectives  43.9 us (14%)
  matrix products  16.7 us (5%)
  local copies, waits for them, and re-layouts  15.8 us (5%)
  between operations  14.1 us (4%)
  other arithmetic  9.15 us (3%)
  starting transfers between devices  5.29 us (2%)
    reduce_scatter x1, waiting for transfers between devices, dense_mix(): lax.psum_scatter(partial, ('fs', 'tp'), scatter_dimension=0, tiled=True)  97.8 us
    all_gather x1, waiting for transfers between devices, dense_mix(): lax.all_gather(jnp.concatenate((normed, coded), axis=0), ('fs', 'tp'), ax...  55.9 us
    all_to_all x1, blocking collectives, to_owners(): lax.all_to_all(pieces, ('fs', 'tp'), split_axis=0, concat_axis=0, tiled=T...  43.9 us
    all_gather x2, waiting for transfers between devices, to_owners(): return lax.all_gather(pieces, 'gr', axis=2, tiled=True)  43.5 us
    all_to_all x1, waiting for transfers between devices, to_owners(): lax.all_to_all(pieces, ('fs', 'tp'), split_axis=0, concat_axis=0, tiled=T...  21.5 us
    dot_general x2, matrix products, dot_last(): lax.dot_general(left, right, (((1,), (1,)), ((), ())), preferred_element_...  8.8 us
    dot_general x1, matrix products, dense_mix(): jnp.dot(act, down, preferred_element_type=jnp.float32).astype(jnp.bfloat16)  7.9 us
  transfers between devices with their start and end apart: 6, of which 5 were waited for; matrix products, arithmetic and copies ran while one was open for 9% of the time, Pallas kernels for 0%

profile of v1, /device:TPU:0, one launch (start us, length us, event | category | flops | bytes accessed | tf_op | source)
XLA Modules:
  0.0 323.8 jit_solution(4078553129348858008)
XLA Ops:
  7.2 1.0 convert_bitcast_fusion.1
  8.3 0.9 fusion.9
  10.8 1.2 fusion.4
  12.1 1.2 fusion.5
  13.3 0.9 pad_maximum_fusion.2
  14.6 43.9 %all_to_all.10 = bf16[16,2,64,256]{3,2,1,0:T(8,128)(2,1)S(1)} all-to-all(bf16[16,2,64,256]{3,2,1,0:T(8,128)(2,1)S(1)} %pad_maximum_fusion.1), channel_id=1, replica_groups=mesh['gr'=2,'fs'=4,'tp'=4] {'fs','tp'}, dimensions={0} | all-to-all | bytes 2097152 | tf_op jit(solution)/shard_map/all_to_all | solution.py:13
  59.3 1.5 reshape.162
  60.9 0.9 convert_bitcast_fusion
  61.7 5.1 %all-to-all-start.1 = ((bf16[16,1,64,256]{3,2,1,0:T(8,128)(2,1)}), bf16[16,1,64,256]{3,2,1,0:T(8,128)(2,1)S(1)}, u32[]{:S(2)}, u32[]{:S(2)}) async-start(bf16[16,1,64,256]{3,2,1,0:T(8,128)(2,1)} %convert_bitcast_fusion), calls=%async_computation.1 | async-start | bytes 1048576 | tf_op jit(solution)/shard_map/all_to_all | solution.py:13
  66.9 21.5 %all-to-all-done.1 = bf16[16,1,64,256]{3,2,1,0:T(8,128)(2,1)S(1)} async-done(((bf16[16,1,64,256]{3,2,1,0:T(8,128)(2,1)}), bf16[16,1,64,256]{3,2,1,0:T(8,128)(2,1)S(1)}, u32[]{:S(2)}, u32[]{:S(2)}) %all-to-all-start.1) | async-done | bytes 524320 | tf_op jit(solution)/shard_map/all_to_all | solution.py:13
  88.8 1.2 reshape.164
  90.1 1.2 slice_bitcast_fusion.2
  91.8 55.9 %all-gather.12.cloned.1.call-done = bf16[2176,2048]{1,0:T(8,128)(2,1)} async-done(((bf16[136,2048]{1,0:T(8,128)(2,1)}), bf16[2176,2048]{1,0:T(8,128)(2,1)}) %all-gather.12.cloned.1.call-update) | async-done | bytes 8912912 | tf_op jit(solution)/shard_map/all_gather | solution.py:39
  147.7 1.1 slice.82
  148.8 1.8 constant_dynamic-slice_fusion
  152.1 29.4 %all-gather.6.cloned.1.call-done = bf16[2,256,2048]{2,1,0:T(8,128)(2,1)} async-done(((bf16[2,256,1024]{2,1,0:T(8,128)(2,1)}), bf16[2,256,2048]{2,1,0:T(8,128)(2,1)}) %all-gather.6.cloned.1.call-update) | async-done | bytes 2097168 | tf_op jit(solution)/shard_map/all_gather | solution.py:16
  181.5 8.0 %fusion.14 = f32[2176,512]{1,0:T(8,128)S(1)} fusion(bf16[2176,2048]{1,0:T(8,128)(2,1)} %all-gather.12.cloned.1.call-done, bf16[512,2048]{1,0:T(8,128)(2,1)} %bitcast.84), kind=kOutput, calls=%fused_computation.45 | convolution fusion | flops 4563402752 | bytes 15466496 | tf_op jit(solution)/shard_map/dot_general | solution.py:20
  190.7 14.1 %all-gather.8.cloned.1.call-done = bf16[1,256,2048]{2,1,0:T(8,128)(2,1)} async-done(((bf16[1,256,1024]{2,1,0:T(8,128)(2,1)}), bf16[1,256,2048]{2,1,0:T(8,128)(2,1)}) %all-gather.8.cloned.1.call-update) | async-done | bytes 1048592 | tf_op jit(solution)/shard_map/all_gather | solution.py:16
  204.8 7.9 %convolution_convert_fusion = bf16[2048,2048]{1,0:T(8,128)(2,1)} fusion(bf16[2048,320]{1,0:T(8,128)(2,1)S(1)} %bitcast.88, bf16[64,2048]{1,0:T(8,128)(2,1)S(1)} %bitcast.97, bf16[256,2048]{1,0:T(8,128)(2,1)} %bitcast.89), kind=kOutput, calls=%fused_computation | convolution fusion | flops 2691170304 | bytes 11010048 | tf_op jit(solution)/shard_map/dot_general | solution.py:55
  214.1 1.7 slice_bitcast_fusion
  215.8 1.3 copy.60
  217.1 1.3 copy.61
  218.4 97.8 %reduce-scatter.2.cloned.1.call-done = bf16[128,2048]{1,0:T(8,128)(2,1)} async-done(((bf16[2048,2048]{1,0:T(8,128)(2,1)}), bf16[128,2048]{1,0:T(8,128)(2,1)}) %reduce-scatter.2.cloned.1.call-update) | async-done | bytes 524304 | tf_op jit(solution)/shard_map/reduce_scatter | solution.py:56
  316.3 1.0 copy.75
  (54 shorter events, 8.0 us)
Async XLA Ops:
  7.2 7.0 %copy-start.5 = (f32[256]{0:T(256)S(1)}, f32[256]{0:T(256)}, u32[]{:S(2)}) copy-start(f32[256]{0:T(256)} %param.17) | copy-start | bytes 3076
  7.2 7.0 %copy-start.1 = (f32[16,256,64]{1,2,0:T(8,128)S(1)}, f32[16,256,64]{1,2,0:T(8,128)}, u32[]{:S(2)}) copy-start(f32[16,256,64]{1,2,0:T(8,128)} %param.11) | copy-start | bytes 3145732
  7.2 7.0 %copy-start.2 = (f32[16,256,64]{1,2,0:T(8,128)S(1)}, f32[16,256,64]{1,2,0:T(8,128)}, u32[]{:S(2)}) copy-start(f32[16,256,64]{1,2,0:T(8,128)} %param.12) | copy-start | bytes 3145732
  7.2 82.9 %all-gather.10.cloned.1.call-start = ((), (), s32[]{:S(2)}) async-start(), calls=%async_computation.5 | async-start | bytes 1179648 | tf_op jit(solution)/shard_map/all_gather | solution.py:125
  10.0 137.8 %all-gather.12.cloned.1.call-start = ((), (), s32[]{:S(2)}) async-start(), calls=%async_computation.7 | async-start | bytes 9469952 | tf_op jit(solution)/shard_map/all_gather | solution.py:39
  14.1 167.3 %all-gather.6.cloned.1.call-start = ((), (), s32[]{:S(2)}) async-start(), calls=%async_computation.3 | async-start | bytes 3145728 | tf_op jit(solution)/shard_map/all_gather | solution.py:16
  58.5 2.4 copy-start
  61.7 26.7 %all-to-all-start.1 = ((bf16[16,1,64,256]{3,2,1,0:T(8,128)(2,1)}), bf16[16,1,64,256]{3,2,1,0:T(8,128)(2,1)S(1)}, u32[]{:S(2)}, u32[]{:S(2)}) async-start(bf16[16,1,64,256]{3,2,1,0:T(8,128)(2,1)} %convert_bitcast_fusion), calls=%async_computation.1 | async-start | bytes 1048576 | tf_op jit(solution)/shard_map/all_to_all | solution.py:13
  66.8 137.9 %all-gather.8.cloned.1.call-start = ((), (), s32[]{:S(2)}) async-start(), calls=%async_computation.4 | async-start | bytes 1572864 | tf_op jit(solution)/shard_map/all_gather | solution.py:16
  90.0 226.3 %reduce-scatter.2.cloned.1.call-start = ((), (), s32[]{:S(2)}) async-start(), calls=%async_computation.6 | async-start | bytes 8912896 | tf_op jit(solution)/shard_map/reduce_scatter | solution.py:56
  91.8 112.9 %copy-start.4 = (bf16[8,8,8,256]{3,1,2,0:T(8,128)(2,1)}, bf16[8,8,8,256]{3,1,2,0:T(8,128)(2,1)S(1)}, u32[]{:S(2)}) copy-start(bf16[8,8,8,256]{3,1,2,0:T(8,128)(2,1)S(1)} %copy.64) | copy-start | bytes 786436
  215.8 100.5 %copy-start.3 = (bf16[1,256,2048]{2,1,0:T(8,128)(2,1)S(1)}, bf16[1,256,2048]{2,1,0:T(8,128)(2,1)}, u32[]{:S(2)}) copy-start(bf16[1,256,2048]{2,1,0:T(8,128)(2,1)} %all-gather.8.cloned.1.call-done) | copy-start | bytes 3145732
Sparse Core Ops, SparseCore 0:
  10.7 48.1 all-gather.9
  61.8 85.8 all-gather.11
  149.8 31.5 all-gather.5
  183.4 21.2 all-gather.7
  212.8 103.4 reduce-scatter.1

commit v2 on v1

--- a/solution.py
+++ b/solution.py
@@ -12,8 +12,17 @@
     fs, tp = lax.axis_size("fs"), lax.axis_size("tp")
     pieces = lax.all_to_all(pieces, ("fs", "tp"), split_axis=0, concat_axis=0, tiled=True)
     pieces = pieces.reshape(fs, tp, kinds, hidden_part, width_part)
-    pieces = pieces.transpose(2, 1, 3, 0, 4).reshape(kinds, tp * hidden_part, fs * width_part)
-    return lax.all_gather(pieces, "gr", axis=2, tiled=True)
+    return pieces.transpose(2, 1, 3, 0, 4).reshape(kinds * tp * hidden_part, fs * width_part)
+
+
+def join_groups(pieces):
+    if lax.axis_size("gr") != 2:
+        return lax.all_gather(pieces, "gr", axis=1, tiled=True)
+    other = lax.ppermute(pieces, "gr", [(0, 1), (1, 0)])
+    first = lax.axis_index("gr") == 0
+    return jnp.concatenate(
+        (jnp.where(first, pieces, other), jnp.where(first, other, pieces)), axis=1
+    )
 
 
 def dot_last(left, right):
@@ -113,17 +122,17 @@
     gained_gate = jnp.swapaxes(train_gate, 1, 2) * norm_gain
     gained_up = jnp.swapaxes(train_up, 1, 2) * norm_gain
     stacked = to_owners(jnp.stack((gained_gate, gained_up), axis=1).astype(jnp.bfloat16))
+    stacked = join_groups(stacked).reshape(2, -1, prompt.shape[1])
     lowered = to_owners(train_down.astype(jnp.bfloat16)[:, None])
-    shared = jnp.stack(
-        (
-            train_shared_gate.T * norm_gain,
-            train_shared_up.T * norm_gain,
-            train_shared_down,
-            jnp.zeros_like(train_shared_down),
-        )
+    shared = jnp.concatenate(
+        (train_shared_gate.T * norm_gain, train_shared_up.T * norm_gain, train_shared_down)
     ).astype(jnp.bfloat16)
-    shared = lax.all_gather(shared, ("gr", "fs"), axis=0)
-    shared = shared[:, :3].transpose(1, 2, 0, 3).reshape(3, train_shared_down.shape[0], -1)
+    shared = jnp.broadcast_to(shared[None], (lax.axis_size("fs"),) + shared.shape)
+    shared = lax.all_to_all(shared, "fs", split_axis=0, concat_axis=0, tiled=True)
+    shared = shared.transpose(1, 0, 2).reshape(shared.shape[1], -1)
+    rest = join_groups(jnp.concatenate((lowered, shared), axis=0))
+    lowered = rest[None, : lowered.shape[0]]
+    shared = rest[lowered.shape[1] :].reshape(3, -1, prompt.shape[1])
     model_width = prompt.shape[1]
     mix = dense_mix if lax.axis_size("fs") * lax.axis_size("tp") <= 2 * expert_ids.shape[1] else sparse_mix
     mixed_out = mix(

time: 324 us -> 275 us (0.85)
  blocking collectives: 43.9 us -> 0 us
  waiting for transfers between devices: 219 us -> 201 us
  starting transfers between devices: 5.29 us -> 19.2 us
  other arithmetic: 9.15 us -> 14.9 us
  matrix products: 16.7 us -> 12.5 us
  local copies, waits for them, and re-layouts: 15.8 us -> 12.2 us
    all_gather x1, waiting for transfers between devices: 55.9 us -> 0.01 us  [dense_mix(): lax.all_gather(jnp.concatenate((normed, coded), axis=0), ('fs', 'tp'), ax...]
    all_to_all x1 -> x0, blocking collectives: 43.9 us -> none  [to_owners(): lax.all_to_all(pieces, ('fs', 'tp'), split_axis=0, concat_axis=0, tiled=T...]
    all_gather x3 -> x0, waiting for transfers between devices: 43.5 us -> none  [the longest x2 43.5 us: to_owners(): return lax.all_gather(pieces, 'gr', axis=2, tiled=True)]
    all_to_all x1 -> x2, waiting for transfers between devices: 21.5 us -> 51.9 us  [to_owners(): lax.all_to_all(pieces, ('fs', 'tp'), split_axis=0, concat_axis=0, tiled=T...]
    ppermute x0 -> x2, waiting for transfers between devices: none -> 19.9 us  [join_groups(): other = lax.ppermute(pieces, 'gr', [(0, 1), (1, 0)])]
    all_to_all x0 -> x1, waiting for transfers between devices: none -> 18.5 us  [body(): lax.all_to_all(shared, 'fs', split_axis=0, concat_axis=0, tiled=True)]
    reduce_scatter x1, waiting for transfers between devices: 97.8 us -> 111 us  [dense_mix(): lax.psum_scatter(partial, ('fs', 'tp'), scatter_dimension=0, tiled=True)]
    all_to_all x0 -> x1, starting transfers between devices: none -> 6.35 us  [body(): lax.all_to_all(shared, 'fs', split_axis=0, concat_axis=0, tiled=True)]
  transfers between devices with their start and end apart: 6 -> 7, of which waited for: 5 -> 5; matrix products, arithmetic and copies ran while one was open for 9% -> 6% of each run, Pallas kernels for 0% -> 0%
where the time goes in v2:
time: 275 us; the launch traced here: 274 us
  waiting for transfers between devices  201 us (73%)
  starting transfers between devices  19.2 us (7%)
  other arithmetic  14.9 us (5%)
  between operations  14.5 us (5%)
  matrix products  12.5 us (5%)
  local copies, waits for them, and re-layouts  12.2 us (4%)
    reduce_scatter x1, waiting for transfers between devices, dense_mix(): lax.psum_scatter(partial, ('fs', 'tp'), scatter_dimension=0, tiled=True)  111 us
    all_to_all x2, waiting for transfers between devices, to_owners(): lax.all_to_all(pieces, ('fs', 'tp'), split_axis=0, concat_axis=0, tiled=T...  51.9 us
    ppermute x2, waiting for transfers between devices, join_groups(): other = lax.ppermute(pieces, 'gr', [(0, 1), (1, 0)])  19.9 us
    all_to_all x1, waiting for transfers between devices, body(): lax.all_to_all(shared, 'fs', split_axis=0, concat_axis=0, tiled=True)  18.5 us
    all_to_all x2, starting transfers between devices, to_owners(): lax.all_to_all(pieces, ('fs', 'tp'), split_axis=0, concat_axis=0, tiled=T...  9.63 us
    unnamed x34, local copies, waits for them, and re-layouts  6.95 us
    dot_general x1, matrix products, dense_mix(): jnp.dot(act, down, preferred_element_type=jnp.float32).astype(jnp.bfloat16)  6.79 us
    all_to_all x1, starting transfers between devices, body(): lax.all_to_all(shared, 'fs', split_axis=0, concat_axis=0, tiled=True)  6.35 us
  transfers between devices with their start and end apart: 7, of which 5 were waited for; matrix products, arithmetic and copies ran while one was open for 6% of the time, Pallas kernels for 0%

profile of v2, /device:TPU:0, one launch (start us, length us, event | category | flops | bytes accessed | tf_op | source)
XLA Modules:
  0.0 274.2 jit_solution(587691433276179100)
XLA Ops:
  8.1 1.2 fusion.5
  9.3 1.3 fusion.6
  12.4 6.3 %all-to-all-start.2 = ((bf16[4,192,256]{2,1,0:T(8,128)(2,1)}), bf16[4,192,256]{2,1,0:T(8,128)(2,1)S(1)}, u32[]{:S(2)}, u32[]{:S(2)}) async-start(bf16[4,192,256]{2,1,0:T(8,128)(2,1)} %broadcast_in_dim.17), calls=%async_computation.2 | async-start | bytes 786432 | tf_op jit(solution)/shard_map/all_to_all | solution.py:131
  19.6 18.5 %all-to-all-done.2 = bf16[4,192,256]{2,1,0:T(8,128)(2,1)S(1)} async-done(((bf16[4,192,256]{2,1,0:T(8,128)(2,1)}), bf16[4,192,256]{2,1,0:T(8,128)(2,1)S(1)}, u32[]{:S(2)}, u32[]{:S(2)}) %all-to-all-start.2) | async-done | bytes 393248 | tf_op jit(solution)/shard_map/all_to_all | solution.py:131
  38.1 4.8 %all-to-all-start.1 = ((bf16[16,1,64,256]{3,2,1,0:T(8,128)(2,1)}), bf16[16,1,64,256]{3,2,1,0:T(8,128)(2,1)S(1)}, u32[]{:S(2)}, u32[]{:S(2)}) async-start(bf16[16,1,64,256]{3,2,1,0:T(8,128)(2,1)} %convert_bitcast_fusion), calls=%async_computation.1 | async-start | bytes 1048576 | tf_op jit(solution)/shard_map/all_to_all | solution.py:13
  43.1 1.1 pad_maximum_fusion.3
  44.2 14.2 %all-to-all-done.1 = bf16[16,1,64,256]{3,2,1,0:T(8,128)(2,1)S(1)} async-done(((bf16[16,1,64,256]{3,2,1,0:T(8,128)(2,1)}), bf16[16,1,64,256]{3,2,1,0:T(8,128)(2,1)S(1)}, u32[]{:S(2)}, u32[]{:S(2)}) %all-to-all-start.1) | async-done | bytes 524320 | tf_op jit(solution)/shard_map/all_to_all | solution.py:13
  58.3 4.8 %all-to-all-start = ((bf16[16,2,64,256]{3,2,1,0:T(8,128)(2,1)}), bf16[16,2,64,256]{3,2,1,0:T(8,128)(2,1)S(1)}, u32[]{:S(2)}, u32[]{:S(2)}) async-start(bf16[16,2,64,256]{3,2,1,0:T(8,128)(2,1)} %pad_maximum_fusion.3), calls=%async_computation | async-start | bytes 2097152 | tf_op jit(solution)/shard_map/all_to_all | solution.py:13
  63.9 1.6 collective-permute-start.1
  65.4 37.7 %all-to-all-done = bf16[16,2,64,256]{3,2,1,0:T(8,128)(2,1)S(1)} async-done(((bf16[16,2,64,256]{3,2,1,0:T(8,128)(2,1)}), bf16[16,2,64,256]{3,2,1,0:T(8,128)(2,1)S(1)}, u32[]{:S(2)}, u32[]{:S(2)}) %all-to-all-start) | async-done | bytes 1048608 | tf_op jit(solution)/shard_map/all_to_all | solution.py:13
  104.2 1.6 collective-permute-start
  105.8 1.6 broadcast_select_fusion.2
  108.2 1.1 fusion.7
  109.2 19.9 %collective-permute-done = bf16[512,1024]{1,0:T(8,128)(2,1)} collective-permute-done((bf16[512,1024]{1,0:T(8,128)(2,1)S(1)}, bf16[512,1024]{1,0:T(8,128)(2,1)}, u32[]{:S(2)}, u32[]{:S(2)}) %collective-permute-start) | collective-permute-done | bytes 1048608 | tf_op jit(solution)/shard_map/ppermute | solution.py:21
  129.1 2.7 broadcast_select_fusion
  131.8 1.1 slice.101
  132.9 1.9 constant_dynamic-slice_fusion
  137.8 4.9 %fusion = f32[2176,512]{1,0:T(8,128)S(1)} fusion(bf16[2176,2048]{1,0:T(8,128)(2,1)S(1)} %copy-done.7, bf16[512,1024]{1,0:T(8,128)(2,1)S(1)} %copy-done, bf16[512,1024]{1,0:T(8,128)(2,1)S(1)} %copy-done.1), kind=kOutput, calls=%fused_computation.15 | convolution fusion | flops 4567597056 | bytes 15466496 | tf_op jit(solution)/shard_map/dot_general | solution.py:29
  144.0 1.0 copy-done.6
  145.0 6.8 %convolution_convert_fusion = bf16[2048,2048]{1,0:T(8,128)(2,1)} fusion(bf16[2048,320]{1,0:T(8,128)(2,1)S(1)} %bitcast.73, bf16[64,2048]{1,0:T(8,128)(2,1)S(1)} %get-tuple-element.39, bf16[256,2048]{1,0:T(8,128)(2,1)S(1)} %copy-done.6), kind=kOutput, calls=%fused_computation | convolution fusion | flops 2691170304 | bytes 11010048 | tf_op jit(solution)/shard_map/dot_general | solution.py:64
  151.8 1.2 fusion.11
  153.0 2.3 copy.46
  155.3 1.3 copy.47
  156.6 110.8 %reduce-scatter.2.cloned.1.call-done = bf16[128,2048]{1,0:T(8,128)(2,1)} async-done(((bf16[2048,2048]{1,0:T(8,128)(2,1)}), bf16[128,2048]{1,0:T(8,128)(2,1)}) %reduce-scatter.2.cloned.1.call-update) | async-done | bytes 524304 | tf_op jit(solution)/shard_map/reduce_scatter | solution.py:65
  (64 shorter events, 10.4 us)
Async XLA Ops:
  7.2 4.3 %copy-start.11 = (f32[64,256]{1,0:T(8,128)S(1)}, f32[64,256]{1,0:T(8,128)}, u32[]{:S(2)}) copy-start(f32[64,256]{1,0:T(8,128)} %param.16) | copy-start | bytes 196612
  7.2 4.3 %copy-start.9 = (f32[256,64]{0,1:T(8,128)S(1)}, f32[256,64]{0,1:T(8,128)}, u32[]{:S(2)}) copy-start(f32[256,64]{0,1:T(8,128)} %param.14) | copy-start | bytes 196612
  7.2 4.3 %copy-start.10 = (f32[256,64]{0,1:T(8,128)S(1)}, f32[256,64]{0,1:T(8,128)}, u32[]{:S(2)}) copy-start(f32[256,64]{0,1:T(8,128)} %param.15) | copy-start | bytes 196612
  7.2 4.3 %copy-start.12 = (f32[256]{0:T(256)S(1)}, f32[256]{0:T(256)}, u32[]{:S(2)}) copy-start(f32[256]{0:T(256)} %param.17) | copy-start | bytes 3076
  7.2 124.6 %all-gather.3.cloned.1.call-start = ((), (), s32[]{:S(2)}) async-start(), calls=%async_computation.5 | async-start | bytes 9469952 | tf_op jit(solution)/shard_map/all_gather | solution.py:48
  9.3 9.4 %copy-start.3 = (f32[16,64,256]{2,1,0:T(8,128)S(1)}, f32[16,64,256]{2,1,0:T(8,128)}, u32[]{:S(2)}) copy-start(f32[16,64,256]{2,1,0:T(8,128)} %param.13) | copy-start | bytes 3145732
  11.6 31.3 %copy-start.4 = (f32[16,256,64]{1,2,0:T(8,128)S(1)}, f32[16,256,64]{1,2,0:T(8,128)}, u32[]{:S(2)}) copy-start(f32[16,256,64]{1,2,0:T(8,128)} %param.11) | copy-start | bytes 3145732
  11.6 31.3 %copy-start.5 = (f32[16,256,64]{1,2,0:T(8,128)S(1)}, f32[16,256,64]{1,2,0:T(8,128)}, u32[]{:S(2)}) copy-start(f32[16,256,64]{1,2,0:T(8,128)} %param.12) | copy-start | bytes 3145732
  12.4 25.7 %all-to-all-start.2 = ((bf16[4,192,256]{2,1,0:T(8,128)(2,1)}), bf16[4,192,256]{2,1,0:T(8,128)(2,1)S(1)}, u32[]{:S(2)}, u32[]{:S(2)}) async-start(bf16[4,192,256]{2,1,0:T(8,128)(2,1)} %broadcast_in_dim.17), calls=%async_computation.2 | async-start | bytes 786432 | tf_op jit(solution)/shard_map/all_to_all | solution.py:131
  38.1 20.3 %all-to-all-start.1 = ((bf16[16,1,64,256]{3,2,1,0:T(8,128)(2,1)}), bf16[16,1,64,256]{3,2,1,0:T(8,128)(2,1)S(1)}, u32[]{:S(2)}, u32[]{:S(2)}) async-start(bf16[16,1,64,256]{3,2,1,0:T(8,128)(2,1)} %convert_bitcast_fusion), calls=%async_computation.1 | async-start | bytes 1048576 | tf_op jit(solution)/shard_map/all_to_all | solution.py:13
  58.3 44.8 %all-to-all-start = ((bf16[16,2,64,256]{3,2,1,0:T(8,128)(2,1)}), bf16[16,2,64,256]{3,2,1,0:T(8,128)(2,1)S(1)}, u32[]{:S(2)}, u32[]{:S(2)}) async-start(bf16[16,2,64,256]{3,2,1,0:T(8,128)(2,1)} %pad_maximum_fusion.3), calls=%async_computation | async-start | bytes 2097152 | tf_op jit(solution)/shard_map/all_to_all | solution.py:13
  63.2 204.2 %reduce-scatter.2.cloned.1.call-start = ((), (), s32[]{:S(2)}) async-start(), calls=%async_computation.4 | async-start | bytes 8912896 | tf_op jit(solution)/shard_map/reduce_scatter | solution.py:65
  63.9 40.3 %copy-start.2 = (bf16[448,1024]{1,0:T(8,128)(2,1)}, bf16[448,1024]{1,0:T(8,128)(2,1)S(1)}, u32[]{:S(2)}) copy-start(bf16[448,1024]{1,0:T(8,128)(2,1)S(1)} %constant_dynamic-update-slice_fusion) | copy-start | bytes 2752516
  63.9 41.9 %collective-permute-start.1 = (bf16[448,1024]{1,0:T(8,128)(2,1)S(1)}, bf16[448,1024]{1,0:T(8,128)(2,1)}, u32[]{:S(2)}, u32[]{:S(2)}) collective-permute-start(bf16[448,1024]{1,0:T(8,128)(2,1)S(1)} %constant_dynamic-update-slice_fusion), channel_id=1, source_target_pairs={{0,16},{16,0},{1,17},{17,1},{2,18},{18,2},{3,19},{19,3},{4,20},{20... | collective-permute-start | bytes 2752520 | tf_op jit(solution)/shard_map/ppermute | solution.py:21
  104.2 24.9 %collective-permute-start = (bf16[512,1024]{1,0:T(8,128)(2,1)S(1)}, bf16[512,1024]{1,0:T(8,128)(2,1)}, u32[]{:S(2)}, u32[]{:S(2)}) collective-permute-start(bf16[512,1024]{1,0:T(8,128)(2,1)S(1)} %bitcast.65), channel_id=1, source_target_pairs={{0,16},{16,0},{1,17},{17,1},{2,18},{18,2},{3,19},{19,3},{4,20},{20... | collective-permute-start | bytes 3145736 | tf_op jit(solution)/shard_map/ppermute | solution.py:21
  108.2 35.8 %copy-start.8 = (bf16[64,2048]{1,0:T(8,128)(2,1)}, bf16[64,2048]{1,0:T(8,128)(2,1)S(1)}, u32[]{:S(2)}) copy-start(bf16[64,2048]{1,0:T(8,128)(2,1)S(1)} %get-tuple-element.39) | copy-start | bytes 786436
  132.9 4.2 %copy-start.7 = (bf16[2176,2048]{1,0:T(8,128)(2,1)S(1)}, bf16[2176,2048]{1,0:T(8,128)(2,1)}, u32[]{:S(2)}) copy-start(bf16[2176,2048]{1,0:T(8,128)(2,1)} %all-gather.3.cloned.1.call-done) | copy-start | bytes 26738692
  135.6 1.9 copy-start
  135.6 2.2 copy-start.1
  143.8 1.2 copy-start.6
Sparse Core Ops, SparseCore 0:
  11.6 109.4 all-gather.2
  152.0 115.3 reduce-scatter.1
